TPU v7x, 32 devices: a whole 2x2x4 slice. The times are simulated.
32 devices in a mesh: grp: 2 (over y), sp: 4 (over z), tp: 4 (over x, core).
Axes of the slice: x: 2, y: 2, z: 4, core: 2. Of those that a mesh axis runs over, the one named last changes fastest.
Arguments:
- tokens: bfloat16 [2048, 8, 2048], P('sp', 'grp'), parts along dimension 1, may hold values from -48 to 48
- query_weight: bfloat16 [2048, 1024], P(None, 'tp'), may hold values from -2 to 2
- key_weight: bfloat16 [2048, 1024], P(None, 'tp'), may hold values from -2 to 2
- value_weight: bfloat16 [2048, 1024], P(None, 'tp'), may hold values from -3 to 3
- mix_gain: float32 [1024], P('tp'), may hold values from 0.1 to 1.9
- out_weight: bfloat16 [1024, 2048], P('tp'), may hold values from -0.1875 to 0.1875
Outputs:
- mixed: bfloat16 [2048, 8, 2048], P(('sp', 'tp'), 'grp'), parts along dimension 1
There are 2 independent parts, one for each index of `grp`. A program takes and returns all parts, laid end to end along the dimension named above; an argument that names none is the same for every part. Nothing has to cross between parts.
All inputs are finite; a program needn't handle non-finite values.
Results may differ from a plain program's by a relative error of at most 0.02.
Values may be sent and summed in bfloat16 or wider, within the bound.
A program may use at most 128 MiB of HBM per device.

v0:
```python
import functools

import jax
import jax.numpy as jnp
from jax import lax
from jax.experimental import pallas as pl
from jax.experimental.pallas import tpu as pltpu
from jax.sharding import PartitionSpec as P

HEAD_DIM = 64
PATTERNS = ((128, 1), (512, 4), (2048, 16))
REACH = 128
CLASSES = 16
LANES = 128
EPSILON = 1e-06
NEGATIVE = -1e30
GROUPS = 2


def attend_kernel(q_ref, k_ref, v_ref, o_ref, out_sc, top_sc, sum_sc, near_bias, mid_bias, far_bias):
    chunks, _, per_class, width = q_ref.shape
    heads = width // HEAD_DIM
    tile = 16
    near_rows = CLASSES * tile
    mid_rows = 4 * per_class
    span = REACH // per_class
    far_tiles = chunks // span

    def bias_of(diff, window, live):
        return jnp.where((diff >= 0) & (diff <= window) & live, 0.0, NEGATIVE).astype(jnp.float32)

    row = lax.broadcasted_iota(jnp.int32, near_bias.shape[1:], 0)
    col = lax.broadcasted_iota(jnp.int32, near_bias.shape[1:], 1)
    diff = (row % tile - col % tile) * 16 + row // tile - (col % near_rows) // tile
    diff = diff + jnp.where(col < near_rows, near_rows, 0)
    near_bias[0] = bias_of(diff, PATTERNS[0][0], col >= near_rows)
    near_bias[1] = bias_of(diff, PATTERNS[0][0], col >= 0)
    row = lax.broadcasted_iota(jnp.int32, mid_bias.shape[1:], 0)
    col = lax.broadcasted_iota(jnp.int32, mid_bias.shape[1:], 1)
    diff = (row % per_class - col % per_class) * 16
    diff = diff + 4 * (row // per_class - (col % mid_rows) // per_class)
    diff = diff + jnp.where(col < mid_rows, CLASSES * per_class, 0)
    mid_bias[0] = bias_of(diff, PATTERNS[1][0], col >= mid_rows)
    mid_bias[1] = bias_of(diff, PATTERNS[1][0], col >= 0)
    row = lax.broadcasted_iota(jnp.int32, far_bias.shape, 0)
    col = lax.broadcasted_iota(jnp.int32, far_bias.shape, 1)
    far_bias[...] = bias_of(row + REACH - col, REACH, col >= 0)

    lane = lax.broadcasted_iota(jnp.int32, (1, width), 1) // HEAD_DIM
    picks = [jnp.where(lane == h, HEAD_DIM ** -0.5, 0.0).astype(jnp.bfloat16) for h in range(heads)]

    def attend(queries, keys, values, bias):
        outs, tops, sums = [], [], []
        for h in range(heads):
            scores = lax.dot_general(
                queries * picks[h], keys, (((1,), (1,)), ((), ())), preferred_element_type=jnp.float32
            ) + bias
            top = jnp.max(scores, axis=1, keepdims=True)
            raised = jnp.exp(scores - top)
            total = jnp.sum(raised, axis=1, keepdims=True)
            outs.append(jnp.dot(raised.astype(jnp.bfloat16), values, preferred_element_type=jnp.float32))
            tops.append(jnp.broadcast_to(top, outs[-1].shape))
            sums.append(jnp.broadcast_to(total, outs[-1].shape))

        def join(parts):
            whole = parts[0]
            for h in range(1, heads):
                whole = jnp.where(lane == h, parts[h], whole)
            return whole

        return join(outs), join(tops), join(sums)

    def merge_rows(ref, *index):
        block = ref[index]
        return block.reshape(-1, width)

    @pl.loop(0, chunks)
    def near_and_mid(z):
        before = jnp.maximum(z - 1, 0)
        first = jnp.minimum(z, 1)
        for u in range(per_class // tile):
            rows = slice(u * tile, (u + 1) * tile)
            back, back_rows, kind = (before, slice(per_class - tile, per_class), first)
            if u > 0:
                back, back_rows, kind = (z, slice((u - 1) * tile, u * tile), 1)
            queries = q_ref[z, :, rows, :].reshape(near_rows, width)
            keys, values = (
                jnp.concatenate(
                    [
                        ref[back, :, back_rows, :].reshape(near_rows, width),
                        ref[z, :, rows, :].reshape(near_rows, width),
                    ],
                    axis=0,
                )
                for ref in (k_ref, v_ref)
            )
            for ref, part in zip((out_sc, top_sc, sum_sc), attend(queries, keys, values, near_bias[kind])):
                ref[0, z, :, rows, :] = part.reshape(CLASSES, tile, width)
        for r in range(4):
            classes = range(r, CLASSES, 4)
            queries = jnp.concatenate([q_ref[z, c] for c in classes], axis=0)
            keys, values = (
                jnp.concatenate([ref[y, c] for y in (before, z) for c in classes], axis=0)
                for ref in (k_ref, v_ref)
            )
            for ref, part in zip((out_sc, top_sc, sum_sc), attend(queries, keys, values, mid_bias[first])):
                for m, c in enumerate(classes):
                    ref[1, z, c] = part[m * per_class : (m + 1) * per_class]

    @pl.loop(0, CLASSES // 4)
    def far(quad):
        for inner in range(4):
            c = quad * 4 + inner
            for n in range(far_tiles):
                here = slice(n * span, (n + 1) * span)
                reach = slice(max(n - 1, 0) * span, (n + 1) * span)
                queries = q_ref[here, c].reshape(REACH, width)
                keys, values = (ref[reach, c].reshape(-1, width) for ref in (k_ref, v_ref))
                bias = far_bias[...] if n > 0 else far_bias[:, REACH:]
                for ref, part in zip((out_sc, top_sc, sum_sc), attend(queries, keys, values, bias)):
                    ref[2, here, c] = part.reshape(span, per_class, width)

    @pl.loop(0, chunks)
    def mix(z):
        tops = [top_sc[p, z] for p in range(3)]
        highest = jnp.maximum(jnp.maximum(tops[0], tops[1]), tops[2])
        lifts = [jnp.exp(top - highest) for top in tops]
        total = sum(lift * sum_sc[p, z] for p, lift in enumerate(lifts))
        result = sum(lift * out_sc[p, z] for p, lift in enumerate(lifts))
        o_ref[z] = (result / total).astype(o_ref.dtype)


def attend_all(moved, width):
    chunks, batches, _, per_class, triple = moved.shape
    channels = triple // 3
    pairs = channels // width
    if width % 128 == 0:
        operands = (moved, moved, moved)
        starts = (0, pairs, 2 * pairs)
    else:
        operands = tuple(moved[..., i * channels : (i + 1) * channels] for i in range(3))
        starts = (0, 0, 0)
    block = (chunks, None, CLASSES, per_class, width)
    tokens = chunks * CLASSES * per_class
    return pl.pallas_call(
        attend_kernel,
        grid=(batches, pairs),
        in_specs=[
            pl.BlockSpec(block, functools.partial(lambda s, b, i: (0, b, 0, 0, s + i), start)) for start in starts
        ],
        out_specs=pl.BlockSpec(block, lambda b, i: (0, b, 0, 0, i)),
        out_shape=jax.ShapeDtypeStruct((chunks, batches, CLASSES, per_class, channels), jnp.bfloat16),
        scratch_shapes=[pltpu.VMEM((3, chunks, CLASSES, per_class, width), jnp.float32) for _ in range(3)]
        + [
            pltpu.VMEM((2, 256, 512), jnp.float32),
            pltpu.VMEM((2, 4 * per_class, 8 * per_class), jnp.float32),
            pltpu.VMEM((REACH, 2 * REACH), jnp.float32),
        ],
        cost_estimate=pl.CostEstimate(
            flops=tokens * batches * channels * 4 * 900,
            bytes_accessed=tokens * batches * channels * 8,
            transcendentals=tokens * batches * channels // HEAD_DIM * 900,
        ),
    )(*operands)


def project_kernel(weight_count, places, tokens_ref, *refs):
    weight_refs, out_ref, product = refs[:weight_count], refs[weight_count], refs[-1]
    step = pl.program_id(0)
    positions, batch_size, features = tokens_ref.shape
    rows = positions * batch_size
    flat = tokens_ref[...].reshape(rows, features)
    at = pl.ds(pl.multiple_of(step * rows, rows), rows)
    for weight_ref, parts in zip(weight_refs, places):
        total = jnp.dot(flat, weight_ref[...], preferred_element_type=jnp.float32)
        for i, part in enumerate(parts):
            product[part, at, :] = total[:, i * LANES : (i + 1) * LANES]

    @pl.when(step == pl.num_programs(0) - 1)
    def leave():
        per_class = out_ref.shape[2]

        @pl.loop(0, CLASSES)
        def of_class(c):
            for part in range(product.shape[0]):
                for b in range(batch_size):
                    picked = pl.ds(c * batch_size + b, per_class, stride=CLASSES * batch_size)
                    out_ref[b, c, :, part * LANES : (part + 1) * LANES] = product[part, picked, :].astype(out_ref.dtype)


def project(tokens, weights, group, cut):
    seq_rows, batch_size, features = tokens.shape
    columns = cut * len(weights)
    per_class = seq_rows // CLASSES
    block = min(64, seq_rows)
    shape = (batch_size, CLASSES, per_class, columns)
    each = cut // LANES
    places = [range(w * each, (w + 1) * each) for w in range(len(weights))]
    return pl.pallas_call(
        functools.partial(project_kernel, len(weights), places),
        grid=(seq_rows // block,),
        in_specs=[pl.BlockSpec((block, batch_size, features), lambda i: (i, 0, 0))]
        + [pl.BlockSpec((features, cut), lambda i: (0, group))] * len(weights),
        out_specs=pl.BlockSpec(shape, lambda i: (0, 0, 0, 0)),
        out_shape=jax.ShapeDtypeStruct(shape, jnp.bfloat16),
        scratch_shapes=[pltpu.VMEM((columns // LANES, seq_rows * batch_size, LANES), jnp.float32)],
        compiler_params=pltpu.CompilerParams(dimension_semantics=("arbitrary",)),
        cost_estimate=pl.CostEstimate(
            flops=2 * seq_rows * batch_size * features * columns,
            bytes_accessed=2 * (tokens.size + features * columns + seq_rows * batch_size * columns),
            transcendentals=0,
        ),
    )(tokens, *weights)


def body(tokens, query_weight, key_weight, value_weight, mix_gain, out_weight):
    seq_rows, batch_size, features = tokens.shape
    channels = query_weight.shape[1]
    sp_count = lax.axis_size("sp")
    tp_count = lax.axis_size("tp")
    tp_place = lax.axis_index("tp")
    per_class = seq_rows // CLASSES
    head_split = min(max(1, sp_count // batch_size), channels // HEAD_DIM)
    copies = max(1, sp_count // (batch_size * head_split))
    batches = max(1, batch_size // sp_count)
    groups = GROUPS if head_split == 1 else 1

    own = (out_weight.astype(jnp.float32) * mix_gain[:, None]).astype(jnp.bfloat16)
    gathered, sources, step = own, [0], tp_count // 2
    while step:
        route = [(i, i ^ step) for i in range(tp_count)]
        gathered = jnp.concatenate([gathered, lax.ppermute(gathered, "tp", route)], axis=0)
        sources += [s ^ step for s in sources]
        step //= 2

    cut = channels // groups // head_split
    width = min(cut, 2 * HEAD_DIM)
    weights = (query_weight, key_weight, value_weight)
    results = []
    for g in range(groups):
        if cut % LANES == 0 and head_split == 1:
            product = project(tokens, weights, g, cut)
        else:
            spans = [slice(i * cut, (i + 1) * cut) for i in range(g * head_split, (g + 1) * head_split)]
            whole = jnp.concatenate([w[:, span] for span in spans for w in weights], axis=1)
            product = project(tokens, (whole,), 0, whole.shape[1])
        if head_split > 1:
            product = product.reshape(batch_size, seq_rows, head_split, 3 * cut).transpose(0, 2, 1, 3)
        product = product.reshape(sp_count // copies, batches * seq_rows, 3 * cut)
        if copies > 1:
            product = jnp.repeat(product, copies, axis=0)
        moved = lax.all_to_all(product, "sp", split_axis=0, concat_axis=0, tiled=True)
        if g == 0:
            moved, gathered = lax.optimization_barrier((moved, gathered))
        moved = moved.reshape(sp_count, batches, CLASSES, per_class, 3 * cut)
        results.append(attend_all(moved, width))

    part = per_class // tp_count
    backs = []
    for result in results:
        back = result.reshape(sp_count, batches, CLASSES, tp_count, part, cut).transpose(0, 3, 1, 2, 4, 5)
        back = back.reshape(sp_count * tp_count, batches * CLASSES * part, cut)
        back = lax.all_to_all(back, ("sp", "tp"), split_axis=0, concat_axis=0, tiled=True)
        back = back.reshape(batch_size // batches, head_split, copies, tp_count, batches, CLASSES, part, cut)[:, :, 0]
        backs.append(back)
    combined = jnp.stack(backs, axis=0).transpose(3, 6, 5, 1, 4, 0, 2, 7)
    rows = part * CLASSES * batch_size
    combined = combined.reshape(tp_count, rows, channels)
    turned = jnp.concatenate(
        [lax.dynamic_index_in_dim(combined, tp_place ^ s, axis=0, keepdims=False) for s in sources], axis=1
    )
    wide = turned.astype(jnp.float32)
    row_scale = lax.rsqrt(jnp.mean(wide * wide, axis=-1, keepdims=True) + EPSILON)
    mixed = jnp.dot(turned, gathered, preferred_element_type=jnp.float32) * row_scale
    return mixed.astype(jnp.bfloat16).reshape(part * CLASSES, batch_size, out_weight.shape[1])


def solution(mesh):
    in_specs = (
        P("sp", "grp", None),
        P(None, "tp"),
        P(None, "tp"),
        P(None, "tp"),
        P("tp"),
        P("tp", None),
    )
    out_specs = P(("sp", "tp"), "grp", None)
    return jax.shard_map(body, mesh=mesh, in_specs=in_specs, out_specs=out_specs, check_vma=False)
```

profile of v0, /device:TPU:0, one launch (start us, length us, event | category | flops | bytes accessed | tf_op | source)
XLA Modules:
  0.0 157.6 jit_solution(17482887396283003568)
XLA Ops:
  0.0 13.5 %shard_map.66 = bf16[4,16,32,384]{3,2,1,0:T(8,128)(2,1)} custom-call(bf16[512,4,2048]{2,1,0:T(4,128)(2,1)} %tokens_ref.3, bf16[2048,256]{1,0:T(8,128)(2,1)} %refs_0_.3, bf16[2048,256]{1,0:T(8,128)(2,1)} %refs_1_.3, bf16[2048,256]{1,0:T(8,128)(2,1)} %refs_2_.3), custom_call_target="tpu_custom_call" | custom-call | flops 3221225472 | bytes 11534336 | tf_op jit(solution)/shard_map/pallas_call | solution.py:199
  13.5 0.0 copy-start
  13.5 0.0 copy-start.1
  13.5 6.5 %all-to-all-start.2 = ((bf16[4,512,384]{2,1,0:T(8,128)(2,1)}), bf16[4,512,384]{2,1,0:T(8,128)(2,1)}, u32[]{:S(2)}, u32[]{:S(2)}) async-start(bf16[4,512,384]{2,1,0:T(8,128)(2,1)} %bitcast.28), calls=%async_computation.2 | async-start | bytes 3145728 | tf_op jit(solution)/shard_map/all_to_all | solution.py:252
  20.0 0.0 copy-done
  20.0 0.0 copy-done.1
  20.0 0.2 multiply_convert_fusion.1
  20.2 1.6 collective-permute-start
  21.8 13.5 %shard_map.64 = bf16[4,16,32,384]{3,2,1,0:T(8,128)(2,1)} custom-call(bf16[512,4,2048]{2,1,0:T(4,128)(2,1)} %tokens_ref.3, bf16[2048,256]{1,0:T(8,128)(2,1)} %refs_0_.3, bf16[2048,256]{1,0:T(8,128)(2,1)} %refs_1_.3, bf16[2048,256]{1,0:T(8,128)(2,1)} %refs_2_.3), custom_call_target="tpu_custom_call" | custom-call | flops 3221225472 | bytes 11534336 | tf_op jit(solution)/shard_map/pallas_call | solution.py:199
  35.2 21.8 %all-to-all-done.2 = bf16[4,512,384]{2,1,0:T(8,128)(2,1)} async-done(((bf16[4,512,384]{2,1,0:T(8,128)(2,1)}), bf16[4,512,384]{2,1,0:T(8,128)(2,1)}, u32[]{:S(2)}, u32[]{:S(2)}) %all-to-all-start.2) | async-done | bytes 1572896 | tf_op jit(solution)/shard_map/all_to_all | solution.py:252
  57.0 4.4 %all-to-all-start = ((bf16[4,512,384]{2,1,0:T(8,128)(2,1)}), bf16[4,512,384]{2,1,0:T(8,128)(2,1)}, u32[]{:S(2)}, u32[]{:S(2)}) async-start(bf16[4,512,384]{2,1,0:T(8,128)(2,1)} %bitcast.27), calls=%async_computation | async-start | bytes 3145728 | tf_op jit(solution)/shard_map/all_to_all | solution.py:252
  61.4 0.0 collective-permute-done
  61.4 1.5 pad_maximum_fusion.1
  62.9 0.0 collective-permute-start.1
  62.9 18.7 %shard_map.67 = bf16[4,1,16,32,128]{4,3,2,1,0:T(8,128)(2,1)} custom-call(bf16[4,1,16,32,384]{4,3,2,1,0:T(8,128)(2,1)} %bitcast.7.q_ref.k_ref.v_ref, bf16[4,1,16,32,384]{4,3,2,1,0:T(8,128)(2,1)} %bitcast.7.q_ref.k_ref.v_ref, bf16[4,1,16,32,384]{4,3,2,1,0:T(8,128)(2,1)} %bitcast.7.q_ref.k_ref.v_ref), custom_call_target="tpu_custom_call" | custom-call | flops 943718400 | bytes 2097152 | tf_op jit(solution)/shard_map/pallas_call | solution.py:145
  81.6 2.0 %copy.8 = bf16[4,1,16,4,8,128]{5,4,2,3,0,1:T(8,128)(2,1)} copy(bf16[4,1,16,4,8,128]{5,4,3,2,0,1:T(8,128)(2,1)} %bitcast.31) | data formatting | bytes 1048576 | tf_op jit(solution)/shard_map/reshape | solution.py:261
  83.6 14.3 %all-to-all-done = bf16[4,512,384]{2,1,0:T(8,128)(2,1)} async-done(((bf16[4,512,384]{2,1,0:T(8,128)(2,1)}), bf16[4,512,384]{2,1,0:T(8,128)(2,1)}, u32[]{:S(2)}, u32[]{:S(2)}) %all-to-all-start) | async-done | bytes 1572896 | tf_op jit(solution)/shard_map/all_to_all | solution.py:252
  98.0 3.8 %all-to-all-start.3 = ((bf16[16,128,128]{2,1,0:T(8,128)(2,1)}), bf16[16,128,128]{2,1,0:T(8,128)(2,1)S(1)}, u32[]{:S(2)}, u32[]{:S(2)}) async-start(bf16[16,128,128]{2,1,0:T(8,128)(2,1)} %bitcast.10), calls=%async_computation.3 | async-start | bytes 1048576 | tf_op jit(solution)/shard_map/all_to_all | solution.py:263
  101.8 0.0 collective-permute-done.1
  101.8 3.4 %pad_maximum_fusion = bf16[1024,2048]{1,0:T(8,128)(2,1)} fusion(bf16[512,2048]{1,0:T(8,128)(2,1)} %collective-permute-done.1, bf16[256,2048]{1,0:T(8,128)(2,1)S(1)} %collective-permute-done, bf16[256,2048]{1,0:T(8,128)(2,1)S(1)} %multiply_convert_fusion.1), kind=kLoop, calls=%fused_computation | loop fusion | flops 12582912 | bytes 8388608 | tf_op jit(solution)/shard_map/concatenate | solution.py:232
  105.2 18.7 %shard_map.65 = bf16[4,1,16,32,128]{4,3,2,1,0:T(8,128)(2,1)} custom-call(bf16[4,1,16,32,384]{4,3,2,1,0:T(8,128)(2,1)} %bitcast.1.q_ref.k_ref.v_ref, bf16[4,1,16,32,384]{4,3,2,1,0:T(8,128)(2,1)} %bitcast.1.q_ref.k_ref.v_ref, bf16[4,1,16,32,384]{4,3,2,1,0:T(8,128)(2,1)} %bitcast.1.q_ref.k_ref.v_ref), custom_call_target="tpu_custom_call" | custom-call | flops 943718400 | bytes 2097152 | tf_op jit(solution)/shard_map/pallas_call | solution.py:145
  123.9 2.0 %copy.7 = bf16[4,1,16,4,8,128]{5,4,2,3,0,1:T(8,128)(2,1)} copy(bf16[4,1,16,4,8,128]{5,4,3,2,0,1:T(8,128)(2,1)} %bitcast.32) | data formatting | bytes 1048576 | tf_op jit(solution)/shard_map/reshape | solution.py:261
  125.9 0.0 all-to-all-done.3
  125.9 6.0 %all-to-all-start.1 = ((bf16[16,128,128]{2,1,0:T(8,128)(2,1)}), bf16[16,128,128]{2,1,0:T(8,128)(2,1)S(1)}, u32[]{:S(2)}, u32[]{:S(2)}) async-start(bf16[16,128,128]{2,1,0:T(8,128)(2,1)} %bitcast.4), calls=%async_computation.1 | async-start | bytes 1048576 | tf_op jit(solution)/shard_map/all_to_all | solution.py:263
  132.0 1.1 copy.10
  133.1 13.2 %all-to-all-done.1 = bf16[16,128,128]{2,1,0:T(8,128)(2,1)S(1)} async-done(((bf16[16,128,128]{2,1,0:T(8,128)(2,1)}), bf16[16,128,128]{2,1,0:T(8,128)(2,1)S(1)}, u32[]{:S(2)}, u32[]{:S(2)}) %all-to-all-start.1) | async-done | bytes 524320 | tf_op jit(solution)/shard_map/all_to_all | solution.py:263
  146.2 1.1 copy.9
  147.3 2.4 %maximum_bitcast_fusion = bf16[4,8,16,4,1,2,1,128]{7,5,3,2,1,0,6,4:T(2,128)(2,1)S(1)} fusion(bf16[1,4,1,4,1,16,8,128]{7,0,1,5,6,3,2,4:T(2,128)(2,1)S(1)} %copy.10, bf16[1,4,1,4,1,16,8,128]{7,0,1,5,6,3,2,4:T(2,128)(2,1)S(1)} %copy.9), kind=kLoop, calls=%fused_computation.5 | loop fusion | flops 2097152 | bytes 2097152 | tf_op jit(solution)/shard_map/transpose | solution.py:266
  149.7 0.7 reshape.47
  150.5 0.1 dynamic-slice_bitcast_fusion.3
  150.5 0.3 multiply_reduce_fusion
  150.8 4.5 %multiply_convert_fusion = bf16[512,2048]{1,0:T(8,128)(2,1)S(1)} fusion(bf16[1024,2048]{1,0:T(8,128)(2,1)} %pad_maximum_fusion, f32[512]{0:T(512)S(1)} %add_rsqrt_fusion, bf16[512,256]{1,0:T(8,128)(2,1)S(1)} %get-tuple-element.10, bf16[512,256]{1,0:T(8,128)(2,1)S(1)} %get-tuple-element.11, bf16[512,256]{1,0:T(8,128)(2,1)S(1)} %get-tuple-element.12, ...), kind=kOutput, calls=%fused_computation.1 | convolution fusion | flops 2153775104 | bytes 7342080 | tf_op jit(solution)/shard_map/dot_general | solution.py:274
  155.4 2.2 %reshape.48 = bf16[128,4,2048]{2,1,0:T(4,128)(2,1)} reshape(bf16[512,2048]{1,0:T(8,128)(2,1)S(1)} %multiply_convert_fusion) | data formatting | bytes 4194304 | tf_op jit(solution)/shard_map/reshape | solution.py:275
  (1 shorter events, 0.0 us)
Async XLA Ops:
  13.5 6.5 %copy-start = (bf16[256,2048]{1,0:T(8,128)(2,1)S(1)}, bf16[256,2048]{1,0:T(8,128)(2,1)}, u32[]{:S(2)}) copy-start(bf16[256,2048]{1,0:T(8,128)(2,1)} %param.11) | copy-start | bytes 3145732
  13.5 6.5 %copy-start.1 = (f32[256]{0:T(256)S(1)}, f32[256]{0:T(256)}, u32[]{:S(2)}) copy-start(f32[256]{0:T(256)} %param.10) | copy-start | bytes 3076
  13.5 43.5 %all-to-all-start.2 = ((bf16[4,512,384]{2,1,0:T(8,128)(2,1)}), bf16[4,512,384]{2,1,0:T(8,128)(2,1)}, u32[]{:S(2)}, u32[]{:S(2)}) async-start(bf16[4,512,384]{2,1,0:T(8,128)(2,1)} %bitcast.28), calls=%async_computation.2 | async-start | bytes 3145728 | tf_op jit(solution)/shard_map/all_to_all | solution.py:252
  20.2 41.2 %collective-permute-start = (bf16[256,2048]{1,0:T(8,128)(2,1)S(1)}, bf16[256,2048]{1,0:T(8,128)(2,1)S(1)}, u32[]{:S(2)}, u32[]{:S(2)}) collective-permute-start(bf16[256,2048]{1,0:T(8,128)(2,1)S(1)} %multiply_convert_fusion.1), channel_id=1, source_target_pairs={{0,2},{1,3},{2,0},{3,1},{4,6},{5,7},{6,4},{7,5},{8,10},{9,11},{10,... | collective-permute-start | bytes 3145736 | tf_op jit(solution)/shard_map/ppermute | solution.py:232
  57.0 40.9 %all-to-all-start = ((bf16[4,512,384]{2,1,0:T(8,128)(2,1)}), bf16[4,512,384]{2,1,0:T(8,128)(2,1)}, u32[]{:S(2)}, u32[]{:S(2)}) async-start(bf16[4,512,384]{2,1,0:T(8,128)(2,1)} %bitcast.27), calls=%async_computation | async-start | bytes 3145728 | tf_op jit(solution)/shard_map/all_to_all | solution.py:252
  62.9 38.9 %collective-permute-start.1 = (bf16[512,2048]{1,0:T(8,128)(2,1)}, bf16[512,2048]{1,0:T(8,128)(2,1)}, u32[]{:S(2)}, u32[]{:S(2)}) collective-permute-start(bf16[512,2048]{1,0:T(8,128)(2,1)} %pad_maximum_fusion.1), channel_id=1, source_target_pairs={{0,1},{1,0},{2,3},{3,2},{4,5},{5,4},{6,7},{7,6},{8,9},{9,8},{10,11... | collective-permute-start | bytes 6291464 | tf_op jit(solution)/shard_map/ppermute | solution.py:232
  98.0 27.9 %all-to-all-start.3 = ((bf16[16,128,128]{2,1,0:T(8,128)(2,1)}), bf16[16,128,128]{2,1,0:T(8,128)(2,1)S(1)}, u32[]{:S(2)}, u32[]{:S(2)}) async-start(bf16[16,128,128]{2,1,0:T(8,128)(2,1)} %bitcast.10), calls=%async_computation.3 | async-start | bytes 1048576 | tf_op jit(solution)/shard_map/all_to_all | solution.py:263
  125.9 20.3 %all-to-all-start.1 = ((bf16[16,128,128]{2,1,0:T(8,128)(2,1)}), bf16[16,128,128]{2,1,0:T(8,128)(2,1)S(1)}, u32[]{:S(2)}, u32[]{:S(2)}) async-start(bf16[16,128,128]{2,1,0:T(8,128)(2,1)} %bitcast.4), calls=%async_computation.1 | async-start | bytes 1048576 | tf_op jit(solution)/shard_map/all_to_all | solution.py:263
where the time goes:
time: 159 us; the launch traced here: 158 us
  Pallas kernels  64.4 us (41%)
  waiting for transfers between devices  49.3 us (31%)
  starting transfers between devices  22.2 us (14%)
  local copies, waits for them, and re-layouts  9.14 us (6%)
  other arithmetic  7.86 us (5%)
  matrix products  4.55 us (3%)
    pallas_call x2, Pallas kernels, attend_all(): pl.pallas_call(attend_kernel, grid=(batches, pairs), in_specs=[pl.BlockSp...  37.5 us
    all_to_all x2, waiting for transfers between devices, body(): lax.all_to_all(product, 'sp', split_axis=0, concat_axis=0, tiled=True)  36.1 us
    pallas_call x2, Pallas kernels, project(): pl.pallas_call(functools.partial(project_kernel, len(weights), places), g...  27 us
    all_to_all x2, waiting for transfers between devices, body(): lax.all_to_all(back, ('sp', 'tp'), split_axis=0, concat_axis=0, tiled=True)  13.2 us
    all_to_all x2, starting transfers between devices, body(): lax.all_to_all(product, 'sp', split_axis=0, concat_axis=0, tiled=True)  10.8 us
    all_to_all x2, starting transfers between devices, body(): lax.all_to_all(back, ('sp', 'tp'), split_axis=0, concat_axis=0, tiled=True)  9.81 us
    concatenate x2, other arithmetic, body(): jnp.concatenate([gathered, lax.ppermute(gathered, 'tp', route)], axis=0)  4.9 us
    dot_general x1, matrix products, body(): jnp.dot(turned, gathered, preferred_element_type=jnp.float32) * row_scale  4.55 us
  transfers between devices with their start and end apart: 6, of which 3 were waited for; matrix products, arithmetic and copies ran while one was open for 6% of the time, Pallas kernels for 32%

commit v1 on v0

--- a/solution.py
+++ b/solution.py
@@ -213,7 +213,438 @@
     )(tokens, *weights)
 
 
+STRIDE = PATTERNS[1][1]
+MESH = pl.DeviceIdType.MESH
+
+
+def split_kernel(pairs, tokens_ref, *refs):
+    weight_refs, out_ref, product = refs[:3], refs[3], refs[4]
+    step = pl.program_id(0)
+    positions, batch_size, features = tokens_ref.shape
+    rows = positions * batch_size
+    flat = tokens_ref[...].reshape(rows, features)
+    at = pl.ds(pl.multiple_of(step * rows, rows), rows)
+    for which, weight_ref in enumerate(weight_refs):
+        total = jnp.dot(flat, weight_ref[...], preferred_element_type=jnp.float32)
+        for pair in range(pairs):
+            product[which * pairs + pair, at, :] = total[:, pair * LANES : (pair + 1) * LANES]
+
+    @pl.when(step == pl.num_programs(0) - 1)
+    def leave():
+        per = out_ref.shape[2] // STRIDE
+
+        @pl.loop(0, STRIDE)
+        def of_class(r):
+            here = pl.ds(pl.multiple_of(r * per, per), per)
+            for b in range(batch_size):
+                picked = pl.ds(r * batch_size + b, per, stride=STRIDE * batch_size)
+                for which in range(3):
+                    for pair in range(pairs):
+                        out_ref[pair * batch_size + b, which, here, :] = product[
+                            which * pairs + pair, picked, :
+                        ].astype(out_ref.dtype)
+
+
+def split_project(tokens, weights):
+    seq_rows, batch_size, features = tokens.shape
+    channels = weights[0].shape[1]
+    pairs = channels // LANES
+    block = min(64, seq_rows)
+    shape = (pairs * batch_size, 3, seq_rows, LANES)
+    return pl.pallas_call(
+        functools.partial(split_kernel, pairs),
+        grid=(seq_rows // block,),
+        in_specs=[pl.BlockSpec((block, batch_size, features), lambda i: (i, 0, 0))]
+        + [pl.BlockSpec((features, channels), lambda i: (0, 0))] * 3,
+        out_specs=pl.BlockSpec(shape, lambda i: (0, 0, 0, 0)),
+        out_shape=jax.ShapeDtypeStruct(shape, jnp.bfloat16),
+        scratch_shapes=[pltpu.VMEM((3 * pairs, seq_rows * batch_size, LANES), jnp.float32)],
+        compiler_params=pltpu.CompilerParams(dimension_semantics=("arbitrary",)),
+        cost_estimate=pl.CostEstimate(
+            flops=6 * seq_rows * batch_size * features * channels,
+            bytes_accessed=2 * (tokens.size + 3 * features * channels + 3 * seq_rows * batch_size * channels),
+            transcendentals=0,
+        ),
+    )(tokens, *weights)
+
+
+def layer_kernel(pairs, batch_size, qkv_ref, own_ref, out_ref, *scratch):
+    (late_q, last_q, first_kv, back, back_norm, sent, sent_norm, held, held_norm, done, gathered, weights, normed,
+     diag_bias, class_bias, corner_bias, send_sem, recv_sem, part_send, part_recv, w_send, w_recv) = scratch
+    place = lax.axis_index("sp")
+    member = lax.axis_index("tp")
+    pieces = qkv_ref.shape[0]
+    chunk = qkv_ref.shape[2]
+    per = chunk // STRIDE
+    tail = REACH // STRIDE
+    members = gathered.shape[0]
+    share = per // members
+    half = LANES // 2
+
+    barrier = pltpu.get_barrier_semaphore()
+    for other in range(1, 4):
+        pl.semaphore_signal(barrier, inc=1, device_id={"sp": lax.rem(place + other, 4)}, device_id_type=MESH)
+        pl.semaphore_signal(barrier, inc=1, device_id={"tp": member ^ other}, device_id_type=MESH)
+    pl.semaphore_wait(barrier, 6)
+
+    def to_place(kind, i, src, dst, target, axis="sp"):
+        return pltpu.make_async_remote_copy(
+            src_ref=src, dst_ref=dst, send_sem=send_sem.at[kind, i], recv_sem=recv_sem.at[kind, i],
+            device_id={axis: target}, device_id_type=MESH,
+        )
+
+    def copy_kv(i):
+        return to_place(0, i, qkv_ref.at[i, pl.ds(1, 2)], first_kv.at[i], 1)
+
+    def copy_q2(i):
+        return to_place(1, i, qkv_ref.at[i, 0], late_q.at[i], 1)
+
+    def copy_q3(i, target):
+        return to_place(1 + target, i, qkv_ref.at[i, 0], last_q.at[i], target)
+
+    def copy_back(i, slot, source_slot, target):
+        kind = 4 + target - 2 + 2 * slot
+        return (
+            to_place(kind, i, sent.at[source_slot, i], back.at[slot, i], target),
+            to_place(kind + 4, i, sent_norm.at[source_slot, i], back_norm.at[slot, i], target),
+        )
+
+    def copy_part(i, x):
+        rows = pl.ds(pl.multiple_of((member ^ x) * share, share), share)
+        return pltpu.make_async_remote_copy(
+            src_ref=done.at[i, :, rows], dst_ref=gathered.at[member, i],
+            send_sem=part_send.at[x - 1, i], recv_sem=part_recv.at[x - 1, i],
+            device_id={"tp": member ^ x}, device_id_type=MESH,
+        )
+
+    def copy_weight(x, kind):
+        src = own_ref if kind < 2 else weights.at[member ^ 2]
+        dst = weights.at[member ^ 2 if kind == 2 else member]
+        return pltpu.make_async_remote_copy(
+            src_ref=src, dst_ref=dst, send_sem=w_send.at[kind], recv_sem=w_recv.at[kind],
+            device_id={"tp": member ^ x}, device_id_type=MESH,
+        )
+
+    @pl.when(place == 0)
+    def send_first():
+        @pl.loop(0, pieces)
+        def one(i):
+            copy_kv(i).start()
+
+    @pl.when(place == 2)
+    def send_late():
+        @pl.loop(0, pieces)
+        def one(i):
+            copy_q2(i).start()
+
+    @pl.when(place == 3)
+    def send_last():
+        @pl.loop(0, pieces)
+        def one(i):
+            copy_q3(i, 1).start()
+            copy_q3(i, 2).start()
+
+    copy_weight(2, 0).start()
+    copy_weight(1, 1).start()
+
+    def bias_of(diff, patterns):
+        count = jnp.zeros(diff.shape, jnp.int32)
+        for window, dilation in patterns:
+            count += jnp.where((diff >= 0) & (diff <= window) & (diff % dilation == 0), 1, 0)
+        logs = jnp.where(count == 2, 0.6931471805599453, jnp.where(count == 3, 1.0986122886681098, 0.0))
+        return jnp.where(count == 0, NEGATIVE, logs).astype(jnp.float32)
+
+    row = lax.broadcasted_iota(jnp.int32, (chunk, LANES), 0)
+    col = lax.broadcasted_iota(jnp.int32, (chunk, LANES), 1)
+    for r in range(STRIDE):
+        diag_bias[r] = bias_of(STRIDE * (col - row % per) + r - row // per, PATTERNS)
+        key = row[:REACH]
+        back_by = STRIDE * (per - tail + key % tail) + key // tail
+        corner_bias[r] = bias_of(chunk + STRIDE * col[:REACH] + r - back_by, PATTERNS[:1])
+    for gap in range(2):
+        class_bias[gap] = bias_of((gap + 1) * chunk + STRIDE * (col[:per] - row[:per]), PATTERNS[1:])
+
+    lane = lax.broadcasted_iota(jnp.int32, (1, LANES), 1) // HEAD_DIM
+    picks = [jnp.where(lane == h, HEAD_DIM ** -0.5, 0.0).astype(jnp.bfloat16) for h in range(2)]
+    eye = jnp.where(
+        lax.broadcasted_iota(jnp.int32, (LANES, LANES), 0) == lax.broadcasted_iota(jnp.int32, (LANES, LANES), 1), 1.0, 0.0
+    ).astype(jnp.bfloat16)
+
+    def contract_last(a, b):
+        return lax.dot_general(a, b, (((1,), (1,)), ((), ())), preferred_element_type=jnp.float32)
+
+    def turn(a):
+        return contract_last(eye, a).astype(jnp.bfloat16)
+
+    def spread(two):
+        return jnp.concatenate([jnp.broadcast_to(two[h : h + 1], (half, LANES)) for h in range(2)], axis=0)
+
+    def attend(queries, parts):
+        both = jnp.concatenate([queries * picks[0], queries * picks[1]], axis=0)
+        scores = []
+        for keys, _, bias in parts:
+            scores.append(contract_last(keys, both) + jnp.concatenate([bias, bias], axis=1))
+        top = functools.reduce(jnp.maximum, [jnp.max(s, axis=0, keepdims=True) for s in scores])
+        total, result = 0.0, 0.0
+        for s, (_, turned, _) in zip(scores, parts):
+            raised = jnp.exp(s - top)
+            total += jnp.sum(raised, axis=0, keepdims=True)
+            result += jnp.dot(turned, raised.astype(jnp.bfloat16), preferred_element_type=jnp.float32)
+        picked = jnp.concatenate([result[:half, :LANES], result[half:, LANES:]], axis=0)
+        norm = top + jnp.log(total)
+        inverse = 1.0 / total
+        two = jnp.concatenate([inverse[:, :LANES], inverse[:, LANES:]], axis=0)
+        return picked * spread(two), jnp.concatenate([norm[:, :LANES], norm[:, LANES:]], axis=0)
+
+    def cls(r):
+        return slice(r * per, (r + 1) * per)
+
+    def corner_of(rows):
+        return jnp.concatenate([rows[r * per + per - tail : (r + 1) * per] for r in range(STRIDE)], axis=0)
+
+    def finish(i, r, result):
+        done[i, r] = turn(result.astype(jnp.bfloat16)[...].reshape(LANES, LANES)).astype(jnp.bfloat16)
+
+    def send_parts(i):
+        mine = pl.ds(pl.multiple_of(member * share, share), share)
+        gathered[member, i] = done[i, :, mine]
+        for x in range(1, members):
+            copy_part(i, x).start()
+
+    def own_parts(i):
+        return qkv_ref[i, 1], turn(qkv_ref[i, 2])
+
+    def far_parts(keys, turned, r, gap):
+        return keys[cls(r)], turned[:, cls(r)], class_bias[gap]
+
+    def give_back(i, source_slot, slot, target, r, answer):
+        sent[source_slot, i, :, cls(r)] = answer[0].astype(jnp.bfloat16)
+        sent_norm[source_slot, i, :, cls(r)] = answer[1]
+
+    def merge(i, sources):
+        for r in range(STRIDE):
+            norms = [held_norm[i, :, cls(r)]] + [back_norm[s, i, :, cls(r)] for s in sources]
+            results = [held[i, :, cls(r)]] + [back[s, i, :, cls(r)].astype(jnp.float32) for s in sources]
+            top = functools.reduce(jnp.maximum, norms)
+            raised = [jnp.exp(n - top) for n in norms]
+            inverse = 1.0 / sum(raised)
+            finish(i, r, sum(spread(e * inverse) * o for e, o in zip(raised, results)))
+
+    @pl.when(place == 0)
+    def first():
+        @pl.loop(0, pieces)
+        def one(i):
+            keys, turned = own_parts(i)
+            for r in range(STRIDE):
+                finish(i, r, attend(qkv_ref[i, 0, cls(r)], [(keys, turned, diag_bias[r])])[0])
+            send_parts(i)
+
+        @pl.loop(0, pieces)
+        def sent_all(i):
+            copy_kv(i).wait_send()
+
+    @pl.when(place == 1)
+    def second():
+        @pl.loop(0, pieces)
+        def one(i):
+            keys, turned = own_parts(i)
+            near_keys = corner_of(keys)
+            near_turned = turn(corner_of(qkv_ref[i, 2]))
+            copy_kv(i).wait_recv()
+            old_keys, old_turned = first_kv[i, 0], turn(first_kv[i, 1])
+            copy_q2(i).wait_recv()
+            for r in range(STRIDE):
+                parts = [
+                    far_parts(keys, turned, r, 0),
+                    (near_keys, near_turned, corner_bias[r]),
+                    far_parts(old_keys, old_turned, r, 1),
+                ]
+                give_back(i, 0, 0, 2, r, attend(late_q[i, cls(r)], parts))
+            for c in copy_back(i, 0, 0, 2):
+                c.start()
+            copy_q3(i, 1).wait_recv()
+            for r in range(STRIDE):
+                parts = [far_parts(keys, turned, r, 1), far_parts(old_keys, old_turned, r, 1)]
+                give_back(i, 1, 0, 3, r, attend(last_q[i, cls(r)], parts))
+            for c in copy_back(i, 0, 1, 3):
+                c.start()
+            old_near_keys = corner_of(old_keys)
+            old_near_turned = turn(corner_of(first_kv[i, 1]))
+            for r in range(STRIDE):
+                parts = [
+                    (keys, turned, diag_bias[r]),
+                    far_parts(old_keys, old_turned, r, 0),
+                    (old_near_keys, old_near_turned, corner_bias[r]),
+                ]
+                finish(i, r, attend(qkv_ref[i, 0, cls(r)], parts)[0])
+            send_parts(i)
+
+        @pl.loop(0, pieces)
+        def sent_all(i):
+            for c in copy_back(i, 0, 0, 2) + copy_back(i, 0, 1, 3):
+                c.wait_send()
+
+    @pl.when(place >= 2)
+    def later():
+        @pl.loop(0, pieces)
+        def one(i):
+            keys, turned = own_parts(i)
+            for r in range(STRIDE):
+                held[i, :, cls(r)], held_norm[i, :, cls(r)] = attend(
+                    qkv_ref[i, 0, cls(r)], [(keys, turned, diag_bias[r])]
+                )
+
+            @pl.when(place == 2)
+            def help_last():
+                near_keys = corner_of(qkv_ref[i, 1])
+                near_turned = turn(corner_of(qkv_ref[i, 2]))
+                copy_q3(i, 2).wait_recv()
+                for r in range(STRIDE):
+                    parts = [far_parts(keys, turned, r, 0), (near_keys, near_turned, corner_bias[r])]
+                    give_back(i, 0, 1, 3, r, attend(last_q[i, cls(r)], parts))
+                for c in copy_back(i, 1, 0, 3):
+                    c.start()
+
+    copy_weight(2, 0).wait_recv()
+    copy_weight(1, 2).start()
+
+    @pl.when(place == 2)
+    def third():
+        @pl.loop(0, pieces)
+        def one(i):
+            for c in copy_back(i, 0, 0, 2):
+                c.wait_recv()
+            merge(i, (0,))
+            send_parts(i)
+
+        @pl.loop(0, pieces)
+        def sent_all(i):
+            copy_q2(i).wait_send()
+            for c in copy_back(i, 1, 0, 3):
+                c.wait_send()
+
+    @pl.when(place == 3)
+    def fourth():
+        @pl.loop(0, pieces)
+        def one(i):
+            for c in copy_back(i, 0, 1, 3) + copy_back(i, 1, 0, 3):
+                c.wait_recv()
+            merge(i, (0, 1))
+            send_parts(i)
+
+        @pl.loop(0, pieces)
+        def sent_all(i):
+            copy_q3(i, 1).wait_send()
+            copy_q3(i, 2).wait_send()
+
+    @pl.loop(0, pieces)
+    def parts_all(i):
+        for x in range(1, members):
+            copy_part(i, x).wait_send()
+            copy_part(i, x).wait_recv()
+
+    copy_weight(1, 1).wait_recv()
+    copy_weight(1, 2).wait_recv()
+    for x, kind in ((2, 0), (1, 1), (1, 2)):
+        copy_weight(x, kind).wait_send()
+    weights[member] = own_ref[...]
+
+    rows = batch_size * STRIDE * share
+    width = pairs * LANES
+    blocks = [gathered[t, p * batch_size : (p + 1) * batch_size].reshape(rows, LANES)
+              for t in range(members) for p in range(pairs)]
+    target = lax.broadcasted_iota(jnp.int32, (rows, rows), 0)
+    source = lax.broadcasted_iota(jnp.int32, (rows, rows), 1)
+    moved_to = (source % share) * (STRIDE * batch_size) + (source // share % STRIDE) * batch_size
+    moved_to = moved_to + source // (share * STRIDE)
+    order = jnp.where(target == moved_to, 1.0, 0.0).astype(jnp.bfloat16)
+    square = 0.0
+    turned = []
+    for block in blocks:
+        turned.append(jnp.dot(order, block, preferred_element_type=jnp.float32))
+        square += turned[-1] * turned[-1]
+    square = jnp.sum(square, axis=1, keepdims=True)
+    scale = lax.rsqrt(square * (1.0 / (LANES * len(blocks))) + EPSILON)
+    for at, block in enumerate(turned):
+        normed[:, at * LANES : (at + 1) * LANES] = (block * scale).astype(jnp.bfloat16)
+
+    @pl.loop(0, out_ref.shape[1] // (2 * LANES))
+    def project_out(n):
+        columns = pl.ds(pl.multiple_of(n * 2 * LANES, 2 * LANES), 2 * LANES)
+        total = 0.0
+        for t in range(members):
+            total += jnp.dot(
+                normed[:, t * width : (t + 1) * width], weights[t, :, columns], preferred_element_type=jnp.float32
+            )
+        out_ref[:, columns] = total.astype(out_ref.dtype)
+
+
+def layer(qkv, own, batch_size, members):
+    pieces, _, chunk, _ = qkv.shape
+    depth, columns = own.shape
+    pairs = pieces // batch_size
+    per = chunk // STRIDE
+    rows = batch_size * chunk // members
+    bf16, f32 = jnp.bfloat16, jnp.float32
+    sems = pltpu.SemaphoreType.DMA
+    return pl.pallas_call(
+        functools.partial(layer_kernel, pairs, batch_size),
+        in_specs=[pl.BlockSpec(memory_space=pltpu.VMEM)] * 2,
+        out_specs=pl.BlockSpec(memory_space=pltpu.VMEM),
+        out_shape=jax.ShapeDtypeStruct((rows, columns), bf16),
+        scratch_shapes=[
+            pltpu.VMEM((pieces, chunk, LANES), bf16),
+            pltpu.VMEM((pieces, chunk, LANES), bf16),
+            pltpu.VMEM((pieces, 2, chunk, LANES), bf16),
+            pltpu.VMEM((2, pieces, LANES, chunk), bf16),
+            pltpu.VMEM((2, pieces, 2, chunk), f32),
+            pltpu.VMEM((2, pieces, LANES, chunk), bf16),
+            pltpu.VMEM((2, pieces, 2, chunk), f32),
+            pltpu.VMEM((pieces, LANES, chunk), f32),
+            pltpu.VMEM((pieces, 2, chunk), f32),
+            pltpu.VMEM((pieces, STRIDE, per, LANES), bf16),
+            pltpu.VMEM((members, pieces, STRIDE, per // members, LANES), bf16),
+            pltpu.VMEM((members, depth, columns), bf16),
+            pltpu.VMEM((rows, depth * members), bf16),
+            pltpu.VMEM((STRIDE, chunk, LANES), f32),
+            pltpu.VMEM((2, per, LANES), f32),
+            pltpu.VMEM((STRIDE, REACH, LANES), f32),
+            sems((12, pieces)),
+            sems((12, pieces)),
+            sems((members - 1, pieces)),
+            sems((members - 1, pieces)),
+            sems((3,)),
+            sems((3,)),
+        ],
+        compiler_params=pltpu.CompilerParams(collective_id=0, has_side_effects=True),
+        cost_estimate=pl.CostEstimate(
+            flops=2 * rows * columns * depth * members, bytes_accessed=2 * qkv.size, transcendentals=qkv.size * 100
+        ),
+    )(qkv, own)
+
+
+def four_chunks(tokens, query_weight, key_weight, value_weight, mix_gain, out_weight):
+    batch_size = tokens.shape[1]
+    own = (out_weight.astype(jnp.float32) * mix_gain[:, None]).astype(jnp.bfloat16)
+    qkv = split_project(tokens, (query_weight, key_weight, value_weight))
+    mixed = layer(qkv, own, batch_size, lax.axis_size("tp"))
+    return mixed.reshape(-1, batch_size, out_weight.shape[1])
+
+
+def fits_four_chunks(tokens, query_weight):
+    return (
+        lax.axis_size("sp") == 4
+        and lax.axis_size("tp") == 4
+        and tokens.shape[0] == STRIDE * LANES
+        and tokens.shape[0] == PATTERNS[1][0]
+        and 4 * tokens.shape[0] <= PATTERNS[2][0]
+        and query_weight.shape[1] % LANES == 0
+    )
+
+
 def body(tokens, query_weight, key_weight, value_weight, mix_gain, out_weight):
+    if fits_four_chunks(tokens, query_weight):
+        return four_chunks(tokens, query_weight, key_weight, value_weight, mix_gain, out_weight)
     seq_rows, batch_size, features = tokens.shape
     channels = query_weight.shape[1]
     sp_count = lax.axis_size("sp")

time: 159 us -> 95.8 us (0.60)
  the two profiles are of different devices: /device:TPU:0 before, /device:TPU:29 now
where the time goes in v1:
time: 95.8 us; the launch traced here: 94.9 us
  Pallas kernels  88.4 us (92%)
  local copies, waits for them, and re-layouts  4.1 us (4%)
  other arithmetic  2.43 us (3%)
    pallas_call x1, Pallas kernels, layer(): pl.pallas_call(functools.partial(layer_kernel, pairs, batch_size), in_spe...  72.7 us
    pallas_call x1, Pallas kernels, split_project(): pl.pallas_call(functools.partial(split_kernel, pairs), grid=(seq_rows //...  15.7 us
    reshape x1, local copies, waits for them, and re-layouts, four_chunks(): return mixed.reshape(-1, batch_size, out_weight.shape[1])  4.1 us
    convert_element_type x1, other arithmetic, four_chunks(): (out_weight.astype(jnp.float32) * mix_gain[:, None]).astype(jnp.bfloat16)  2.43 us

profile of v1, /device:TPU:29, one launch (start us, length us, event | category | flops | bytes accessed | tf_op | source)
XLA Modules:
  0.0 94.9 jit_solution(184827064582960898)
XLA Ops:
  0.0 2.4 %multiply_convert_fusion.own_ref = bf16[256,2048]{1,0:T(8,128)(2,1)} fusion(bf16[256,2048]{1,0:T(8,128)(2,1)} %param.11, f32[256]{0:T(256)} %param.10), kind=kLoop, calls=%fused_computation | loop fusion | flops 1572864 | bytes 2098176 | tf_op jit(solution)/shard_map/convert_element_type | solution.py:628
  2.4 15.7 %shard_map.64.qkv_ref = bf16[8,3,512,128]{3,2,1,0:T(8,128)(2,1)} custom-call(bf16[512,4,2048]{2,1,0:T(4,128)(2,1)} %tokens_ref.1, bf16[2048,256]{1,0:T(8,128)(2,1)} %refs_0_.1, bf16[2048,256]{1,0:T(8,128)(2,1)} %refs_1_.1, bf16[2048,256]{1,0:T(8,128)(2,1)} %refs_2_.1), custom_call_target="tpu_custom_call" | custom-call | flops 6442450944 | bytes 14680064 | tf_op jit(solution)/shard_map/pallas_call | solution.py:254
  18.1 72.7 %shard_map.65 = bf16[512,2048]{1,0:T(8,128)(2,1)} custom-call(bf16[8,3,512,128]{3,2,1,0:T(8,128)(2,1)} %shard_map.64.qkv_ref, bf16[256,2048]{1,0:T(8,128)(2,1)} %multiply_convert_fusion.own_ref), custom_call_target="tpu_custom_call" | custom-call | flops 2147483648 | bytes 3145728 | tf_op jit(solution)/shard_map/pallas_call | solution.py:590
  90.8 4.1 %reshape.4 = bf16[128,4,2048]{2,1,0:T(4,128)(2,1)} reshape(bf16[512,2048]{1,0:T(8,128)(2,1)} %shard_map.65) | data formatting | bytes 4194304 | tf_op jit(solution)/shard_map/reshape | solution.py:631

commit v2 on v0

--- a/solution.py
+++ b/solution.py
@@ -213,7 +213,507 @@
     )(tokens, *weights)
 
 
+STRIDE = PATTERNS[1][1]
+MESH = pl.DeviceIdType.MESH
+
+
+def layer_kernel(tokens_ref, *refs):
+    in_weights, gain_ref, own_ref, out_ref = refs[:3], refs[3], refs[4], refs[5]
+    (raw, kept, product, qkv_ref, in_sem, late_q, last_q, first_kv, back, back_norm, sent, sent_norm, held, held_norm, done, gathered, weights, gains, normed,
+     mixed, diag_bias, class_bias, corner_bias, send_sem, recv_sem, part_send, part_recv, w_send, w_recv, out_sem) = refs[6:]
+    place = lax.axis_index("sp")
+    member = lax.axis_index("tp")
+    blocks, depth, _, batch_size, features = tokens_ref.shape
+    pieces = qkv_ref.shape[0]
+    pairs = pieces // batch_size
+    per = qkv_ref.shape[3]
+    chunk = per * STRIDE
+    tail = REACH // STRIDE
+    members = gathered.shape[0]
+    share = per // members
+    half = LANES // 2
+
+    def read_tokens(n, slot):
+        return [
+            pltpu.make_async_copy(tokens_ref.at[n, :, r], raw.at[slot, r], in_sem.at[slot, r]) for r in range(STRIDE)
+        ]
+
+    read_weights = [
+        pltpu.make_async_copy(ref, kept.at[:, w * pairs * LANES : (w + 1) * pairs * LANES], in_sem.at[2, w])
+        for w, ref in enumerate(in_weights)
+    ]
+    read_own = pltpu.make_async_copy(own_ref, weights.at[member], in_sem.at[2, 3])
+    for c in read_tokens(0, 0) + read_weights + read_tokens(1, 1) + [read_own]:
+        c.start()
+
+    barrier = pltpu.get_barrier_semaphore()
+    for other in range(1, 4):
+        pl.semaphore_signal(barrier, inc=1, device_id={"sp": lax.rem(place + other, 4)}, device_id_type=MESH)
+        pl.semaphore_signal(barrier, inc=1, device_id={"tp": member ^ other}, device_id_type=MESH)
+    pl.semaphore_wait(barrier, 6)
+
+    def to_place(kind, i, src, dst, target, axis="sp"):
+        return pltpu.make_async_remote_copy(
+            src_ref=src, dst_ref=dst, send_sem=send_sem.at[kind, i], recv_sem=recv_sem.at[kind, i],
+            device_id={axis: target}, device_id_type=MESH,
+        )
+
+    def copy_kv(i, rows=slice(None)):
+        return to_place(0, i, qkv_ref.at[i, pl.ds(1, 2), :, rows], first_kv.at[i, :, :, rows], 1)
+
+    def copy_q2(i, rows=slice(None)):
+        return to_place(1, i, qkv_ref.at[i, 0, :, rows], late_q.at[i, :, rows], 1)
+
+    def copy_q3(i, target, rows=slice(None)):
+        return to_place(1 + target, i, qkv_ref.at[i, 0, :, rows], last_q.at[i, :, rows], target)
+
+    def copy_back(i, slot, source_slot, target):
+        kind = 4 + target - 2 + 2 * slot
+        return (
+            to_place(kind, i, sent.at[source_slot, i], back.at[slot, i], target),
+            to_place(kind + 4, i, sent_norm.at[source_slot, i], back_norm.at[slot, i], target),
+        )
+
+    def copy_part(i, x):
+        rows = pl.ds(pl.multiple_of((member ^ x) * share, share), share)
+        return pltpu.make_async_remote_copy(
+            src_ref=done.at[i, :, rows], dst_ref=gathered.at[member, i],
+            send_sem=part_send.at[x - 1, i], recv_sem=part_recv.at[x - 1, i],
+            device_id={"tp": member ^ x}, device_id_type=MESH,
+        )
+
+    def copy_gain(x):
+        return pltpu.make_async_remote_copy(
+            src_ref=gain_ref, dst_ref=gains.at[member], send_sem=w_send.at[2 + x], recv_sem=w_recv.at[2 + x],
+            device_id={"tp": member ^ x}, device_id_type=MESH,
+        )
+
+    def copy_weight(x, kind):
+        src = own_ref if kind < 2 else weights.at[member ^ 2]
+        dst = weights.at[member ^ 2 if kind == 2 else member]
+        return pltpu.make_async_remote_copy(
+            src_ref=src, dst_ref=dst, send_sem=w_send.at[kind], recv_sem=w_recv.at[kind],
+            device_id={"tp": member ^ x}, device_id_type=MESH,
+        )
+
+    def send_early(i, rows=slice(None)):
+        @pl.when(place == 0)
+        def send_first():
+            copy_kv(i, rows).start()
+
+        @pl.when(place == 2)
+        def send_late():
+            copy_q2(i, rows).start()
+
+        @pl.when(place == 3)
+        def send_last():
+            copy_q3(i, 1, rows).start()
+            copy_q3(i, 2, rows).start()
+
+    copy_weight(2, 0).start()
+    copy_weight(1, 1).start()
+    for x in range(1, members):
+        copy_gain(x).start()
+
+    def bias_of(diff, patterns):
+        count = jnp.zeros(diff.shape, jnp.int32)
+        for window, dilation in patterns:
+            count += jnp.where((diff >= 0) & (diff <= window) & (diff % dilation == 0), 1, 0)
+        logs = jnp.where(count == 2, 0.6931471805599453, jnp.where(count == 3, 1.0986122886681098, 0.0))
+        return jnp.where(count == 0, NEGATIVE, logs).astype(jnp.float32)
+
+    row = lax.broadcasted_iota(jnp.int32, (chunk, LANES), 0)
+    col = lax.broadcasted_iota(jnp.int32, (chunk, LANES), 1)
+    for r in range(STRIDE):
+        diag_bias[r] = bias_of(STRIDE * (col - row % per) + r - row // per, PATTERNS)
+        key = row[:REACH]
+        back_by = STRIDE * (per - tail + key % tail) + key // tail
+        corner_bias[r] = bias_of(chunk + STRIDE * col[:REACH] + r - back_by, PATTERNS[:1])
+    for gap in range(2):
+        class_bias[gap] = bias_of((gap + 1) * chunk + STRIDE * (col[:per] - row[:per]), PATTERNS[1:])
+
+    early = min(2, pieces)
+    for c in read_weights:
+        c.wait()
+
+    @pl.loop(0, blocks)
+    def project(n):
+        slot = lax.rem(n, 2)
+        for c in read_tokens(n, slot):
+            c.wait()
+        flat = raw[slot].reshape(STRIDE * depth * batch_size, features)
+        total = jnp.dot(flat, kept[...], preferred_element_type=jnp.float32)
+        for part in range(3 * pairs):
+            product[part] = total[:, part * LANES : (part + 1) * LANES]
+
+        @pl.when(n + 2 < blocks)
+        def read_ahead():
+            for c in read_tokens(n + 2, slot):
+                c.start()
+
+        here = pl.ds(pl.multiple_of(n * depth, depth), depth)
+        for b in range(batch_size):
+            for which in range(3):
+                for pair in range(pairs):
+                    for r in range(STRIDE):
+                        picked = pl.ds(r * depth * batch_size + b, depth, stride=batch_size)
+                        qkv_ref[pair * batch_size + b, which, r, here] = product[
+                            which * pairs + pair, picked
+                        ].astype(jnp.bfloat16)
+        for i in range(early):
+            send_early(i, here)
+
+    @pl.loop(early, pieces)
+    def send_rest(i):
+        send_early(i)
+
+    read_own.wait()
+    lane = lax.broadcasted_iota(jnp.int32, (1, LANES), 1) // HEAD_DIM
+    picks = [jnp.where(lane == h, HEAD_DIM ** -0.5, 0.0).astype(jnp.bfloat16) for h in range(2)]
+    eye = jnp.where(
+        lax.broadcasted_iota(jnp.int32, (LANES, LANES), 0) == lax.broadcasted_iota(jnp.int32, (LANES, LANES), 1), 1.0, 0.0
+    ).astype(jnp.bfloat16)
+
+    def contract_last(a, b):
+        return lax.dot_general(a, b, (((1,), (1,)), ((), ())), preferred_element_type=jnp.float32)
+
+    def turn(a):
+        return contract_last(eye, a).astype(jnp.bfloat16)
+
+    def spread(two):
+        return jnp.concatenate([jnp.broadcast_to(two[h : h + 1], (half, LANES)) for h in range(2)], axis=0)
+
+    def attend(jobs):
+        begun = []
+        for queries, parts in jobs:
+            both = jnp.concatenate([queries * picks[0], queries * picks[1]], axis=0)
+            scores = []
+            for keys, _, bias in parts:
+                scores.append(contract_last(keys, both) + jnp.concatenate([bias, bias], axis=1))
+            top = functools.reduce(jnp.maximum, [jnp.max(s, axis=0, keepdims=True) for s in scores])
+            begun.append((scores, top, parts))
+        mixed = []
+        for scores, top, parts in begun:
+            total, result = 0.0, 0.0
+            for s, (_, turned, _) in zip(scores, parts):
+                raised = jnp.exp(s - top)
+                total += jnp.sum(raised, axis=0, keepdims=True)
+                result += jnp.dot(turned, raised.astype(jnp.bfloat16), preferred_element_type=jnp.float32)
+            mixed.append((result, top, total))
+        answers = []
+        for result, top, total in mixed:
+            picked = jnp.concatenate([result[:half, :LANES], result[half:, LANES:]], axis=0)
+            norm = top + jnp.log(total)
+            inverse = 1.0 / total
+            two = jnp.concatenate([inverse[:, :LANES], inverse[:, LANES:]], axis=0)
+            answers.append((picked * spread(two), jnp.concatenate([norm[:, :LANES], norm[:, LANES:]], axis=0)))
+        return answers
+
+    def all_rows(block):
+        return block.reshape(chunk, LANES)
+
+    def cls(r):
+        return slice(r * per, (r + 1) * per)
+
+    def corner_of(rows):
+        return jnp.concatenate([rows[r * per + per - tail : (r + 1) * per] for r in range(STRIDE)], axis=0)
+
+    def finish(i, results):
+        rows = [turn(result.astype(jnp.bfloat16)) for result in results]
+        for r in range(STRIDE):
+            done[i, r] = rows[r]
+
+    def send_parts(i):
+        mine = pl.ds(pl.multiple_of(member * share, share), share)
+        gathered[member, i] = done[i, :, mine]
+        for x in range(1, members):
+            copy_part(i, x).start()
+
+    def own_parts(i):
+        return all_rows(qkv_ref[i, 1]), turn(all_rows(qkv_ref[i, 2]))
+
+    def far_parts(keys, turned, r, gap):
+        return keys[cls(r)], turned[:, cls(r)], class_bias[gap]
+
+    def give_back(i, source_slot, answers):
+        for r in range(STRIDE):
+            sent[source_slot, i, :, cls(r)] = answers[r][0].astype(jnp.bfloat16)
+            sent_norm[source_slot, i, :, cls(r)] = answers[r][1]
+
+    def merge(i, sources):
+        rows = []
+        for r in range(STRIDE):
+            norms = [held_norm[i, :, cls(r)]] + [back_norm[s, i, :, cls(r)] for s in sources]
+            results = [held[i, :, cls(r)]] + [back[s, i, :, cls(r)].astype(jnp.float32) for s in sources]
+            top = functools.reduce(jnp.maximum, norms)
+            raised = [jnp.exp(n - top) for n in norms]
+            inverse = 1.0 / sum(raised)
+            rows.append(sum(spread(e * inverse) * o for e, o in zip(raised, results)))
+        finish(i, rows)
+
+    @pl.when(place >= 2)
+    def later():
+        @pl.loop(0, pieces)
+        def one(i):
+            keys, turned = own_parts(i)
+            jobs = [(qkv_ref[i, 0, r], [(keys, turned, diag_bias[r])]) for r in range(STRIDE)]
+            for r, (result, norm) in enumerate(attend(jobs)):
+                held[i, :, cls(r)] = result
+                held_norm[i, :, cls(r)] = norm
+
+            @pl.when(place == 2)
+            def help_last():
+                near_keys = corner_of(all_rows(qkv_ref[i, 1]))
+                near_turned = turn(corner_of(all_rows(qkv_ref[i, 2])))
+                copy_q3(i, 2).wait_recv()
+                jobs = []
+                for r in range(STRIDE):
+                    parts = [far_parts(keys, turned, r, 0), (near_keys, near_turned, corner_bias[r])]
+                    jobs.append((last_q[i, r], parts))
+                give_back(i, 0, attend(jobs))
+                for c in copy_back(i, 1, 0, 3):
+                    c.start()
+
+    def first(i):
+        keys, turned = own_parts(i)
+        jobs = [(qkv_ref[i, 0, r], [(keys, turned, diag_bias[r])]) for r in range(STRIDE)]
+        finish(i, [answer[0] for answer in attend(jobs)])
+
+    def second(i):
+        keys, turned = own_parts(i)
+        near_keys = corner_of(keys)
+        near_turned = turn(corner_of(all_rows(qkv_ref[i, 2])))
+        copy_kv(i).wait_recv()
+        old_keys, old_turned = all_rows(first_kv[i, 0]), turn(all_rows(first_kv[i, 1]))
+        copy_q2(i).wait_recv()
+        jobs = []
+        for r in range(STRIDE):
+            parts = [
+                far_parts(keys, turned, r, 0),
+                (near_keys, near_turned, corner_bias[r]),
+                far_parts(old_keys, old_turned, r, 1),
+            ]
+            jobs.append((late_q[i, r], parts))
+        give_back(i, 0, attend(jobs))
+        for c in copy_back(i, 0, 0, 2):
+            c.start()
+        copy_q3(i, 1).wait_recv()
+        jobs = []
+        for r in range(STRIDE):
+            parts = [far_parts(keys, turned, r, 1), far_parts(old_keys, old_turned, r, 1)]
+            jobs.append((last_q[i, r], parts))
+        give_back(i, 1, attend(jobs))
+        for c in copy_back(i, 0, 1, 3):
+            c.start()
+        old_near_keys = corner_of(old_keys)
+        old_near_turned = turn(corner_of(all_rows(first_kv[i, 1])))
+        jobs = []
+        for r in range(STRIDE):
+            parts = [
+                (keys, turned, diag_bias[r]),
+                far_parts(old_keys, old_turned, r, 0),
+                (old_near_keys, old_near_turned, corner_bias[r]),
+            ]
+            jobs.append((qkv_ref[i, 0, r], parts))
+        finish(i, [answer[0] for answer in attend(jobs)])
+
+    def third(i):
+        for c in copy_back(i, 0, 0, 2):
+            c.wait_recv()
+        merge(i, (0,))
+
+    def fourth(i):
+        for c in copy_back(i, 0, 1, 3) + copy_back(i, 1, 0, 3):
+            c.wait_recv()
+        merge(i, (0, 1))
+
+    rows = STRIDE * share
+    width = pairs * LANES
+    target = lax.broadcasted_iota(jnp.int32, (rows, rows), 0)
+    source = lax.broadcasted_iota(jnp.int32, (rows, rows), 1)
+    order = jnp.where(target == source % share * STRIDE + source // share, 1.0, 0.0).astype(jnp.bfloat16)
+
+    def write_out(b):
+        return pltpu.make_async_copy(mixed.at[b], out_ref.at[b], out_sem.at[b])
+
+    def project_out(b):
+        for pair in range(pairs):
+            for x in range(1, members):
+                copy_part(pair * batch_size + b, x).wait_recv()
+        square = 0.0
+        turned = []
+        for t in range(members):
+            for pair in range(pairs):
+                block = gathered[t, pair * batch_size + b].reshape(rows, LANES)
+                turned.append(jnp.dot(order, block, preferred_element_type=jnp.float32))
+                square += turned[-1] * turned[-1]
+        square = jnp.sum(square, axis=1, keepdims=True)
+        scale = lax.rsqrt(square * (1.0 / (LANES * len(turned))) + EPSILON)
+        for at, block in enumerate(turned):
+            gain = gains[at // pairs, at % pairs : at % pairs + 1]
+            normed[:, at * LANES : (at + 1) * LANES] = (block * scale * gain).astype(jnp.bfloat16)
+
+        @pl.loop(0, mixed.shape[2] // (2 * LANES))
+        def columns_of(n):
+            columns = pl.ds(pl.multiple_of(n * 2 * LANES, 2 * LANES), 2 * LANES)
+            total = 0.0
+            for t in range(members):
+                total += jnp.dot(
+                    normed[:, t * width : (t + 1) * width], weights[t, :, columns], preferred_element_type=jnp.float32
+                )
+            mixed[b, :, columns] = total.astype(mixed.dtype)
+
+        write_out(b).start()
+
+    ready = (pairs - 1) * batch_size
+
+    @pl.loop(0, pieces)
+    def one(i):
+        for role, complete in enumerate((first, second, third, fourth)):
+            @pl.when(place == role)
+            def run(complete=complete):
+                complete(i)
+        send_parts(i)
+
+        @pl.when(i == pieces // 2 - 1)
+        def forward():
+            copy_weight(2, 0).wait_recv()
+            copy_weight(1, 2).start()
+
+        @pl.when(i == ready)
+        def weights_here():
+            copy_weight(1, 1).wait_recv()
+            copy_weight(1, 2).wait_recv()
+            for x in range(1, members):
+                copy_gain(x).wait_recv()
+            gains[member] = gain_ref[...]
+
+        @pl.when(i > ready)
+        def previous():
+            project_out(i - ready - 1)
+
+    project_out(batch_size - 1)
+
+    @pl.when(place == 0)
+    def first_sent():
+        @pl.loop(0, pieces)
+        def one(i):
+            copy_kv(i).wait_send()
+
+    @pl.when(place == 1)
+    def second_sent():
+        @pl.loop(0, pieces)
+        def one(i):
+            for c in copy_back(i, 0, 0, 2) + copy_back(i, 0, 1, 3):
+                c.wait_send()
+
+    @pl.when(place == 2)
+    def third_sent():
+        @pl.loop(0, pieces)
+        def one(i):
+            copy_q2(i).wait_send()
+            for c in copy_back(i, 1, 0, 3):
+                c.wait_send()
+
+    @pl.when(place == 3)
+    def fourth_sent():
+        @pl.loop(0, pieces)
+        def one(i):
+            copy_q3(i, 1).wait_send()
+            copy_q3(i, 2).wait_send()
+
+    @pl.loop(0, pieces)
+    def parts_sent(i):
+        for x in range(1, members):
+            copy_part(i, x).wait_send()
+
+    for x, kind in ((2, 0), (1, 1), (1, 2)):
+        copy_weight(x, kind).wait_send()
+    for x in range(1, members):
+        copy_gain(x).wait_send()
+    for b in range(batch_size):
+        write_out(b).wait()
+
+
+def four_chunks(tokens, query_weight, key_weight, value_weight, mix_gain, out_weight):
+    chunk, batch_size, features = tokens.shape
+    width, columns = out_weight.shape
+    members = lax.axis_size("tp")
+    pairs = width // LANES
+    pieces = pairs * batch_size
+    per = chunk // STRIDE
+    depth = 16
+    rows = chunk // members
+    bf16, f32 = jnp.bfloat16, jnp.float32
+    sems = pltpu.SemaphoreType.DMA
+    scratch = [
+        pltpu.VMEM((2, STRIDE, depth, batch_size, features), bf16),
+        pltpu.VMEM((features, 3 * width), bf16),
+        pltpu.VMEM((3 * pairs, STRIDE * depth * batch_size, LANES), f32),
+        pltpu.VMEM((pieces, 3, STRIDE, per, LANES), bf16),
+        sems((3, STRIDE)),
+        pltpu.VMEM((pieces, STRIDE, per, LANES), bf16),
+        pltpu.VMEM((pieces, STRIDE, per, LANES), bf16),
+        pltpu.VMEM((pieces, 2, STRIDE, per, LANES), bf16),
+        pltpu.VMEM((2, pieces, LANES, chunk), bf16),
+        pltpu.VMEM((2, pieces, 2, chunk), f32),
+        pltpu.VMEM((2, pieces, LANES, chunk), bf16),
+        pltpu.VMEM((2, pieces, 2, chunk), f32),
+        pltpu.VMEM((pieces, LANES, chunk), f32),
+        pltpu.VMEM((pieces, 2, chunk), f32),
+        pltpu.VMEM((pieces, STRIDE, per, LANES), bf16),
+        pltpu.VMEM((members, pieces, STRIDE, per // members, LANES), bf16),
+        pltpu.VMEM((members, width, columns), bf16),
+        pltpu.VMEM((members, pairs, LANES), f32),
+        pltpu.VMEM((rows, width * members), bf16),
+        pltpu.VMEM((batch_size, rows, columns), bf16),
+        pltpu.VMEM((STRIDE, chunk, LANES), f32),
+        pltpu.VMEM((2, per, LANES), f32),
+        pltpu.VMEM((STRIDE, REACH, LANES), f32),
+        sems((12, pieces)),
+        sems((12, pieces)),
+        sems((members - 1, pieces)),
+        sems((members - 1, pieces)),
+        sems((2 + members,)),
+        sems((2 + members,)),
+        sems((batch_size,)),
+    ]
+    mixed = pl.pallas_call(
+        layer_kernel,
+        in_specs=[pl.BlockSpec(memory_space=pl.ANY)] * 4
+        + [pl.BlockSpec(memory_space=pltpu.VMEM), pl.BlockSpec(memory_space=pl.ANY)],
+        out_specs=pl.BlockSpec(memory_space=pl.ANY),
+        out_shape=jax.ShapeDtypeStruct((batch_size, rows, columns), bf16),
+        scratch_shapes=scratch,
+        compiler_params=pltpu.CompilerParams(collective_id=0, has_side_effects=True),
+        cost_estimate=pl.CostEstimate(
+            flops=6 * tokens.size * width, bytes_accessed=4 * tokens.size, transcendentals=tokens.size * 100
+        ),
+    )(
+        tokens.reshape(per // depth, depth, STRIDE, batch_size, features),
+        query_weight,
+        key_weight,
+        value_weight,
+        mix_gain.reshape(pairs, LANES),
+        out_weight,
+    )
+    return mixed.transpose(1, 0, 2)
+
+
+def fits_four_chunks(tokens, query_weight):
+    return (
+        lax.axis_size("sp") == 4
+        and lax.axis_size("tp") == 4
+        and tokens.shape[0] == STRIDE * LANES
+        and tokens.shape[0] == PATTERNS[1][0]
+        and 4 * tokens.shape[0] <= PATTERNS[2][0]
+        and query_weight.shape[1] % LANES == 0
+    )
+
+
 def body(tokens, query_weight, key_weight, value_weight, mix_gain, out_weight):
+    if fits_four_chunks(tokens, query_weight):
+        return four_chunks(tokens, query_weight, key_weight, value_weight, mix_gain, out_weight)
     seq_rows, batch_size, features = tokens.shape
     channels = query_weight.shape[1]
     sp_count = lax.axis_size("sp")

time: 159 us -> 81.9 us (0.52)
  the two profiles are of different devices: /device:TPU:0 before, /device:TPU:29 now
where the time goes in v2:
time: 81.9 us; the launch traced here: 81.2 us
  Pallas kernels  76.7 us (94%)
  local copies, waits for them, and re-layouts  4.53 us (6%)
    pallas_call x1, Pallas kernels, four_chunks(): pl.pallas_call(layer_kernel, in_specs=[pl.BlockSpec(memory_space=pl.ANY)]...  76.7 us
    transpose x1, local copies, waits for them, and re-layouts, four_chunks(): return mixed.transpose(1, 0, 2)  4.53 us

profile of v2, /device:TPU:29, one launch (start us, length us, event | category | flops | bytes accessed | tf_op | source)
XLA Modules:
  0.0 81.2 jit_solution(15724537372280033823)
XLA Ops:
  0.0 76.7 %shard_map.64 = bf16[4,128,2048]{2,1,0:T(8,128)(2,1)} custom-call(bf16[8,16,4,4,2048]{4,3,2,1,0:T(4,128)(2,1)} %bitcast.4, bf16[2048,256]{1,0:T(8,128)(2,1)} %refs_0_.1, bf16[2048,256]{1,0:T(8,128)(2,1)} %refs_1_.1, bf16[2048,256]{1,0:T(8,128)(2,1)} %refs_2_.1, f32[2,128]{1,0:T(2,128)} %bitcast.5, bf16[256,2048]{1,0:T(8,128)(2,1)} %refs_4_.1), custom_call_target="tpu_custom_call" | custom-call | flops 6442450944 | bytes 16777216 | tf_op jit(solution)/shard_map/pallas_call | solution.py:681
  76.7 4.5 %copy.7 = bf16[128,4,2048]{2,1,0:T(4,128)(2,1)} copy(bf16[128,4,2048]{2,0,1:T(8,128)(2,1)} %bitcast.3) | data formatting | bytes 4194304 | tf_op jit(solution)/shard_map/transpose | solution.py:700
